TPU v7x, 512 devices: a whole 4x8x8 slice. The times are simulated.
512 devices in a mesh: sp: 32 (over z, x), tp: 16 (over y, core).
Axes of the slice: x: 4, y: 8, z: 8, core: 2. Of those that a mesh axis runs over, the one named last changes fastest.
Arguments:
- queries: bfloat16 [8192, 1024], P('sp', 'tp'), may hold values from -64 to 64
- keys: bfloat16 [8192, 1024], P('sp', 'tp'), may hold values from -64 to 64
- values: bfloat16 [8192, 1024], P('sp', 'tp'), may hold values from -6 to 6
- cum_gate: float32 [16, 8192], P('tp'), may hold values from -8192 to 0, as said below
- out_weight: bfloat16 [1024, 2048], P('tp'), may hold values from -0.375 to 0.375
- resid: bfloat16 [8192, 2048], P('sp'), may hold values from -6 to 6
- norm_gain: float32 [2048], replicated, may hold values from 0.1 to 1.9
- routes: int32 [8192, 2], P('sp'), may hold values from 0 to 31, all different within a row; in each aligned block of 256 rows (0 to 255, 256 to 511, ...) at most 20 rows name the same one
- route_weight: float32 [8192, 2], P('sp'), may hold values from 0.1 to 0.9
- gate_weight: bfloat16 [32, 2048, 4096], P('sp', None, 'tp'), may hold values from -0.125 to 0.125
- up_weight: bfloat16 [32, 2048, 4096], P('sp', None, 'tp'), may hold values from -0.125 to 0.125
- down_weight: bfloat16 [32, 4096, 2048], P('sp', 'tp'), may hold values from -0.09375 to 0.09375
Outputs:
- layer_out: bfloat16 [8192, 2048], P('sp', 'tp')
Inputs may be any that keep to these rules, and one draw needn't show every extreme that they name: `routes`: each token names 2 different experts. Among the rows of one index of sp, no expert is named more than 20 times, a bound that some block reaches. `cum_gate`: each head's row does not rise along the positions.
All inputs are finite; a program needn't handle non-finite values.
Results may differ from a plain program's by a relative error of at most 0.015.
Values may be sent and summed in bfloat16 or wider, within the bound.
No kernel may reach another device: no remote copies, remote signals or barrier semaphores. Data moves between devices by JAX's collectives and lax.ppermute only.
A program may use at most 64 MiB of HBM per device.

v0:
```python
import math
import jax
import jax.numpy as jnp
from jax import lax
from jax.sharding import PartitionSpec as P

HD = 64
epsilon = 1e-06


def in_one_piece(arrays, axis, dim, along):
    ends, at = ([], 0)
    for a in arrays[:-1]:
        at += a.shape[along]
        ends.append(at)
    both = jnp.concatenate(arrays, axis=along)
    return tuple(jnp.split(lax.all_gather(both, axis, axis=dim, tiled=True), ends, axis=along))


def in_blocks(x, dim, length):
    before, after = (x.shape[:dim], x.shape[dim + 1 :])
    return jnp.moveaxis(x.reshape(*before, length, -1, *after), dim, 0)


def sum_at_owner(x, axis, dim):
    tiles = in_blocks(x, dim, lax.axis_size(axis))
    arrived = lax.all_to_all(tiles, axis, split_axis=0, concat_axis=0, tiled=True)
    return arrived.astype(jnp.float32).sum(axis=0)


def from_everyone(x, axis):
    length = lax.axis_size(axis)
    return lax.all_to_all(jnp.broadcast_to(x[None], (length, *x.shape)), axis, 0, 0, tiled=True)


def of_everyone(x, axis):
    everything = from_everyone(x, axis)
    return jnp.sum(everything, axis=0)


def attend_block(
    carried, query_heads, cum_query, key_rows, value_rows, cum_keys, query_first, key_first
):
    best_score, weight_sum, value_sum = carried
    score_scale = query_heads.shape[-1] ** (-0.5)
    scores = (
        jnp.einsum("hqd,hkd->hqk", query_heads, key_rows, preferred_element_type=jnp.float32)
        * score_scale
    )
    scores = scores + cum_query[:, :, None] - cum_keys[:, None, :]
    query_pos = query_first + jnp.arange(query_heads.shape[1], dtype=jnp.int32)
    key_pos = key_first + jnp.arange(key_rows.shape[1], dtype=jnp.int32)
    permitted_mask = (key_pos[None, :] <= query_pos[:, None])[None]
    new_best = jnp.maximum(
        best_score, jnp.max(jnp.where(permitted_mask, scores, -jnp.inf), axis=-1)
    )
    weights = jnp.where(permitted_mask, jnp.exp(scores - new_best[..., None]), 0.0)
    shrink = jnp.exp(best_score - new_best)
    weight_sum = weight_sum * shrink + jnp.sum(weights, axis=-1)
    value_sum = value_sum * shrink[..., None] + jnp.einsum(
        "hqk,hkd->hqd", weights.astype(jnp.bfloat16), value_rows, preferred_element_type=jnp.float32
    )
    return (new_best, weight_sum, value_sum)


def local(
    queries,
    keys,
    values,
    cum_gate,
    out_weight,
    resid,
    norm_gain,
    routes,
    route_weight,
    gate_weight,
    up_weight,
    down_weight,
):
    rows_here = queries.shape[0]
    heads_here = queries.shape[1] // HD
    sp_count = lax.axis_size("sp")
    tp_count = lax.axis_size("tp")
    shift_amount = lax.axis_index("sp") * rows_here
    model_width = resid.shape[1]
    columns = model_width // tp_count
    column_first = lax.axis_index("tp") * columns
    query_heads = queries.reshape(rows_here, heads_here, HD).transpose(1, 0, 2)
    cum_query = lax.dynamic_slice_in_dim(cum_gate, shift_amount, rows_here, 1)
    start_state = (
        jnp.full((heads_here, rows_here), -1e30, jnp.float32),
        jnp.zeros((heads_here, rows_here), jnp.float32),
        jnp.zeros((heads_here, rows_here, HD), jnp.float32),
    )
    key_part, value_part = in_one_piece((keys, values), "sp", 0, 1)
    piece_rows = key_part.shape[0]
    key_block = math.gcd(piece_rows, 1024)

    def attend_piece(running):

        def key_step(block_index, inner_state):
            block_first = block_index * key_block
            key_rows = lax.dynamic_slice_in_dim(key_part, block_first, key_block, 0)
            key_rows = key_rows.reshape(key_block, heads_here, HD).transpose(1, 0, 2)
            value_rows = lax.dynamic_slice_in_dim(value_part, block_first, key_block, 0)
            value_rows = value_rows.reshape(key_block, heads_here, HD).transpose(1, 0, 2)
            cum_keys = lax.dynamic_slice_in_dim(cum_gate, block_first, key_block, 1)
            return attend_block(
                inner_state,
                query_heads,
                cum_query,
                key_rows,
                value_rows,
                cum_keys,
                shift_amount,
                block_first,
            )

        return lax.fori_loop(0, piece_rows // key_block, key_step, running)

    best_score, weight_sum, value_sum = lax.cond(
        jnp.int32(0) <= shift_amount + rows_here - 1,
        attend_piece,
        lambda running: running,
        start_state,
    )
    attended = (value_sum / weight_sum[..., None]).astype(jnp.bfloat16)
    attended = attended.transpose(1, 0, 2).reshape(rows_here, heads_here * HD)
    partial_value = jnp.dot(attended, out_weight, preferred_element_type=jnp.float32)
    mixed_sum = sum_at_owner(partial_value.astype(jnp.bfloat16), "tp", 1)
    stream_cols = (
        lax.dynamic_slice_in_dim(resid, column_first, columns, 1).astype(jnp.float32) + mixed_sum
    )
    square_sum = of_everyone(jnp.sum(stream_cols * stream_cols, axis=1, keepdims=True), "tp")
    gain_cols = lax.dynamic_slice_in_dim(norm_gain, column_first, columns, 0)
    normed = (stream_cols * lax.rsqrt(square_sum / model_width + epsilon) * gain_cols).astype(
        jnp.bfloat16
    )
    capacity = 5 * rows_here // (2 * sp_count)
    chosen = routes.reshape(-1)
    onehot = (chosen[:, None] == jnp.arange(sp_count, dtype=jnp.int32)[None, :]).astype(jnp.int32)
    before = jnp.cumsum(onehot, axis=0) - onehot
    rank_within = jnp.sum(before * onehot, axis=1)
    slot_index = chosen * capacity + rank_within
    source_row = (
        jnp.zeros((sp_count * capacity,), jnp.int32)
        .at[slot_index]
        .set(jnp.arange(chosen.shape[0], dtype=jnp.int32) // routes.shape[1])
    )
    filled = jnp.zeros((sp_count * capacity,), jnp.bool_).at[slot_index].set(True)
    outgoing = jnp.where(filled[:, None], normed[source_row], jnp.zeros((), jnp.bfloat16))
    outgoing = outgoing.reshape(sp_count, capacity, normed.shape[1])
    gate_here = gate_weight[0]
    up_here = up_weight[0]
    local_down_weight = down_weight[0]
    arrived = lax.all_to_all(outgoing, "sp", split_axis=0, concat_axis=0, tiled=True)
    arrived_rows = arrived.reshape(-1, columns)
    col_part = lax.all_gather(arrived_rows, "tp", axis=1, tiled=True)
    gate_sum = jnp.dot(col_part, gate_here, preferred_element_type=jnp.float32)
    up_sum = jnp.dot(col_part, up_here, preferred_element_type=jnp.float32)
    slot_shape = arrived.shape
    hidden = (jax.nn.silu(gate_sum) * up_sum).astype(jnp.bfloat16)
    partial_term = jnp.dot(hidden, local_down_weight, preferred_element_type=jnp.float32)
    expert_rows = sum_at_owner(partial_term.astype(jnp.bfloat16), "tp", 1).astype(jnp.bfloat16)
    returned = expert_rows.reshape(slot_shape[0], slot_shape[1], columns)
    returned_back = lax.all_to_all(returned, "sp", split_axis=0, concat_axis=0, tiled=True)
    returned_flat = returned_back.reshape(sp_count * capacity, columns)
    picked = (
        returned_flat[slot_index].reshape(rows_here, routes.shape[1], columns).astype(jnp.float32)
    )
    combined = jnp.sum(picked * route_weight[..., None], axis=1)
    return (stream_cols + combined).astype(jnp.bfloat16)


def solution(mesh):
    return jax.shard_map(
        local,
        mesh=mesh,
        in_specs=(
            P("sp", "tp"),
            P("sp", "tp"),
            P("sp", "tp"),
            P("tp", None),
            P("tp", None),
            P("sp", None),
            P(),
            P("sp", None),
            P("sp", None),
            P("sp", None, "tp"),
            P("sp", None, "tp"),
            P("sp", "tp", None),
        ),
        out_specs=P("sp", "tp"),
        check_vma=False,
    )
```

profile of v0, /device:TPU:1, one launch (start us, length us, event | category | flops | bytes accessed | tf_op | source)
XLA Modules:
  0.0 370.9 jit_solution(9054272636798588638)
XLA Ops:
  9.1 86.0 %all-gather.3.cloned.1.call-done = bf16[8192,128]{1,0:T(8,128)(2,1)} async-done(((bf16[256,128]{1,0:T(8,128)(2,1)}), bf16[8192,128]{1,0:T(8,128)(2,1)}) %all-gather.3.cloned.1.call-update) | async-done | bytes 2097168 | tf_op jit(solution)/shard_map/all_gather | solution.py:17
  95.1 49.2 %conditional.1 = (f32[1,256]{1,0:T(1,128)}, f32[1,256,64]{1,2,0:T(8,128)}) conditional(s32[]{:T(128)} %convert_element_type.51, () %tuple.31, (bf16[8192,128]{1,0:T(8,128)(2,1)}, bf16[256,64]{0,1:T(8,128)(2,1)}, s32[]{:T(128)}, f32[1,8192]{1,0:T(1,128)}) %tuple.32), branch_computations={%region_0.0_spmd, %region_1.6_spmd} | conditional | flops 70830592 | bytes 8277405 | solution.py:121
  95.9 5.0 %fusion.45 = (bf16[8192,64]{1,0:T(8,128)(2,1)}, bf16[8192,64]{1,0:T(8,128)(2,1)}) fusion(bf16[8192,128]{1,0:T(8,128)(2,1)} %get-tuple-element.217), kind=kLoop, calls=%fused_computation.87 | loop fusion | bytes 4194304 | tf_op jit(solution)/shard_map/split | solution.py:17
  101.0 43.3 %while.20 = (s32[]{:T(128)}, f32[1,256]{1,0:T(1,128)S(1)}, f32[1,256]{1,0:T(1,128)}, f32[1,256,64]{1,2,0:T(8,128)}, s32[]{:T(128)}, /*index=5*/bf16[8192,64]{1,0...) while((s32[]{:T(128)}, f32[1,256]{1,0:T(1,128)S(1)}, ...), condition=%wide.region_5.5_spmd.clone, body=%wide.region_2.4_spmd.clone.sunk | while | flops 70830592 | bytes 3884243 | solution.py:119
  103.9 2.0 fusion.62
  109.3 2.0 fusion.62
  112.1 1.4 fusion.58
  114.8 2.0 fusion.62
  117.6 1.4 fusion.58
  120.3 2.0 fusion.62
  125.8 2.0 fusion.62
  131.3 2.0 fusion.62
  134.0 1.4 fusion.58
  136.8 2.0 fusion.62
  142.2 2.0 fusion.62
  146.8 12.3 %all-to-all-start = ((bf16[16,256,128]{2,1,0:T(8,128)(2,1)}), bf16[16,256,128]{2,1,0:T(8,128)(2,1)S(1)}, u32[]{:S(2)}, u32[]{:S(2)}) async-start(bf16[16,256,128]{2,1,0:T(8,128)(2,1)} %bitcast.74), calls=%async_computation | async-start | bytes 2097152 | tf_op jit(solution)/shard_map/all_to_all | solution.py:27
  161.5 2.4 scatter_custom_fusion.1
  164.0 23.2 %all-to-all-done = bf16[16,256,128]{2,1,0:T(8,128)(2,1)S(1)} async-done(((bf16[16,256,128]{2,1,0:T(8,128)(2,1)}), bf16[16,256,128]{2,1,0:T(8,128)(2,1)S(1)}, u32[]{:S(2)}, u32[]{:S(2)}) %all-to-all-start) | async-done | bytes 1048608 | tf_op jit(solution)/shard_map/all_to_all | solution.py:27
  188.9 3.4 all-to-all-start.1
  193.2 2.4 scatter_custom_fusion
  195.7 3.9 %all-to-all-done.1 = f32[16,256,1]{1,2,0:T(1,128)S(1)} async-done(((f32[16,256,1]{1,2,0:T(1,128)}), f32[16,256,1]{1,2,0:T(1,128)S(1)}, u32[]{:S(2)}, u32[]{:S(2)}) %all-to-all-start.1) | async-done | bytes 16416 | tf_op jit(solution)/shard_map/all_to_all | solution.py:33
  200.7 2.0 gather_fusion
  202.9 15.5 %all_to_all.25 = bf16[32,20,128]{2,1,0:T(8,128)(2,1)S(1)} all-to-all(bf16[32,20,128]{2,1,0:T(8,128)(2,1)S(1)} %broadcast_select_fusion.2), channel_id=1, replica_groups=mesh['sp'=32,'tp'=16] {'sp'}, dimensions={0} | all-to-all | bytes 327680 | tf_op jit(solution)/shard_map/all_to_all | solution.py:156
  219.1 38.1 %all-gather.5.cloned.1.call-done = bf16[640,2048]{1,0:T(8,128)(2,1)} async-done(((bf16[640,128]{1,0:T(8,128)(2,1)}), bf16[640,2048]{1,0:T(8,128)(2,1)}) %all-gather.5.cloned.1.call-update) | async-done | bytes 2621456 | tf_op jit(solution)/shard_map/all_gather | solution.py:158
  257.2 3.4 fusion.26
  260.7 6.2 %fusion.21 = bf16[80,16,8,128]{3,2,1,0:T(8,128)(2,1)} fusion(bf16[1,256,2048]{2,1,0:T(8,128)(2,1)S(1)} %copy-done, bf16[640,2048]{1,0:T(8,128)(2,1)} %all-gather.5.cloned.1.call-done, bf16[1,2048,256]{2,1,0:T(8,128)(2,1)S(1)} %copy-done.6, f32[640,256]{1,0:T(8,128)} %fusion.26), kind=kOutput, calls=%fused_computation.40 | convolution fusion | flops 1344471040 | bytes 7995392 | tf_op jit(solution)/shard_map/dot_general | solution.py:163
  266.9 2.4 copy.43
  269.3 67.0 %all_to_all.26 = bf16[16,640,128]{2,1,0:T(8,128)(2,1)} all-to-all(bf16[16,640,128]{2,1,0:T(8,128)(2,1)S(1)} %bitcast.91), channel_id=1, replica_groups=mesh['sp'=32,'tp'=16] {'tp'}, dimensions={0} | all-to-all | bytes 5242880 | tf_op jit(solution)/shard_map/all_to_all | solution.py:27
  336.3 2.1 reduce_sum.77
  339.2 9.9 %all-to-all-start.4 = ((bf16[32,20,128]{2,1,0:T(8,128)(2,1)}), bf16[32,20,128]{2,1,0:T(8,128)(2,1)S(1)}, u32[]{:S(2)}, u32[]{:S(2)}) async-start(bf16[32,20,128]{2,1,0:T(8,128)(2,1)} %reshape.156), calls=%async_computation.4 | async-start | bytes 393216 | tf_op jit(solution)/shard_map/all_to_all | solution.py:166
  349.3 11.5 %all-to-all-done.4 = bf16[32,20,128]{2,1,0:T(8,128)(2,1)S(1)} async-done(((bf16[32,20,128]{2,1,0:T(8,128)(2,1)}), bf16[32,20,128]{2,1,0:T(8,128)(2,1)S(1)}, u32[]{:S(2)}, u32[]{:S(2)}) %all-to-all-start.4) | async-done | bytes 163872 | tf_op jit(solution)/shard_map/all_to_all | solution.py:166
  362.5 1.5 add_convert_fusion
  (123 shorter events, 38.4 us)
Async XLA Ops:
  6.5 254.1 %copy-start = (bf16[1,256,2048]{2,1,0:T(8,128)(2,1)S(1)}, bf16[1,256,2048]{2,1,0:T(8,128)(2,1)}, u32[]{:S(2)}) copy-start(bf16[1,256,2048]{2,1,0:T(8,128)(2,1)} %param.27) | copy-start | bytes 3145732
  6.5 88.6 %all-gather.3.cloned.1.call-start = ((), (), s32[]{:S(2)}) async-start(), calls=%async_computation.5 | async-start | bytes 2162688 | tf_op jit(solution)/shard_map/all_gather | solution.py:17
  95.1 49.2 %copy-start.1 = (bf16[64,2048]{1,0:T(8,128)(2,1)S(1)}, bf16[64,2048]{1,0:T(8,128)(2,1)}, u32[]{:S(2)}) copy-start(bf16[64,2048]{1,0:T(8,128)(2,1)} %param.20) | copy-start | bytes 786436
  95.9 5.0 %copy-start.2 = (bf16[256,64]{0,1:T(8,128)(2,1)S(1)}, bf16[256,64]{0,1:T(8,128)(2,1)}, u32[]{:S(2)}) copy-start(bf16[256,64]{0,1:T(8,128)(2,1)} %get-tuple-element.272) | copy-start | bytes 98308 | tf_op jit(solution)/shard_map/cond
  144.3 14.9 %copy-start.3 = (s32[256,2]{0,1:T(2,128)S(1)}, s32[256,2]{0,1:T(2,128)}, u32[]{:S(2)}) copy-start(s32[256,2]{0,1:T(2,128)} %param.23) | copy-start | bytes 6148
  146.8 40.3 %all-to-all-start = ((bf16[16,256,128]{2,1,0:T(8,128)(2,1)}), bf16[16,256,128]{2,1,0:T(8,128)(2,1)S(1)}, u32[]{:S(2)}, u32[]{:S(2)}) async-start(bf16[16,256,128]{2,1,0:T(8,128)(2,1)} %bitcast.74), calls=%async_computation | async-start | bytes 2097152 | tf_op jit(solution)/shard_map/all_to_all | solution.py:27
  161.1 96.1 %copy-start.5 = (bf16[1,2048,256]{2,1,0:T(8,128)(2,1)S(1)}, bf16[1,2048,256]{2,1,0:T(8,128)(2,1)}, u32[]{:S(2)}) copy-start(bf16[1,2048,256]{2,1,0:T(8,128)(2,1)} %param.25) | copy-start | bytes 3145732
  188.9 10.8 %all-to-all-start.1 = ((f32[16,256,1]{1,2,0:T(1,128)}), f32[16,256,1]{1,2,0:T(1,128)S(1)}, u32[]{:S(2)}, u32[]{:S(2)}) async-start(f32[16,256,1]{1,2,0:T(1,128)} %broadcast_in_dim.90), calls=%async_computation.1 | async-start | bytes 32768 | tf_op jit(solution)/shard_map/all_to_all | solution.py:33
  192.3 64.9 %all-gather.5.cloned.1.call-start = ((), (), s32[]{:S(2)}) async-start(), calls=%async_computation.6 | async-start | bytes 2785280 | tf_op jit(solution)/shard_map/all_gather | solution.py:158
  219.1 41.5 %copy-start.6 = (bf16[1,2048,256]{2,1,0:T(8,128)(2,1)S(1)}, bf16[1,2048,256]{2,1,0:T(8,128)(2,1)}, u32[]{:S(2)}) copy-start(bf16[1,2048,256]{2,1,0:T(8,128)(2,1)} %param.26) | copy-start | bytes 3145732
  336.3 12.8 %copy-start.4 = (f32[256,2]{0,1:T(2,128)S(1)}, f32[256,2]{0,1:T(2,128)}, u32[]{:S(2)}) copy-start(f32[256,2]{0,1:T(2,128)} %param.24) | copy-start | bytes 6148
  339.2 21.5 %all-to-all-start.4 = ((bf16[32,20,128]{2,1,0:T(8,128)(2,1)}), bf16[32,20,128]{2,1,0:T(8,128)(2,1)S(1)}, u32[]{:S(2)}, u32[]{:S(2)}) async-start(bf16[32,20,128]{2,1,0:T(8,128)(2,1)} %reshape.156), calls=%async_computation.4 | async-start | bytes 393216 | tf_op jit(solution)/shard_map/all_to_all | solution.py:166
Sparse Core Ops, SparseCore 0:
  10.5 84.5 all-gather.2
  219.2 37.9 all-gather.4
where the time goes:
time: 372 us; the launch traced here: 371 us
  waiting for transfers between devices  163 us (44%)
  blocking collectives  82.6 us (22%)
  matrix products  38 us (10%)
  local copies, waits for them, and re-layouts  29.2 us (8%)
  starting transfers between devices  25.7 us (7%)
  other arithmetic  19 us (5%)
  between operations  13.6 us (4%)
    all_gather x1, waiting for transfers between devices, in_one_piece(): lax.all_gather(both, axis, axis=dim, tiled=True)  86 us
    all_to_all x1, blocking collectives, sum_at_owner(): lax.all_to_all(tiles, axis, split_axis=0, concat_axis=0, tiled=True)  67 us
    all_gather x1, waiting for transfers between devices, local(): col_part = lax.all_gather(arrived_rows, 'tp', axis=1, tiled=True)  38.1 us
    all_to_all x1, waiting for transfers between devices, sum_at_owner(): lax.all_to_all(tiles, axis, split_axis=0, concat_axis=0, tiled=True)  23.2 us
    dot_general x8, matrix products, attend_block(): jnp.einsum('hqk,hkd->hqd', weights.astype(jnp.bfloat16), value_rows, pref...  16.2 us
    all_to_all x1, blocking collectives, local(): lax.all_to_all(outgoing, 'sp', split_axis=0, concat_axis=0, tiled=True)  15.5 us
    all_to_all x1, starting transfers between devices, sum_at_owner(): lax.all_to_all(tiles, axis, split_axis=0, concat_axis=0, tiled=True)  12.3 us
    all_to_all x1, waiting for transfers between devices, local(): lax.all_to_all(returned, 'sp', split_axis=0, concat_axis=0, tiled=True)  11.5 us
  transfers between devices with their start and end apart: 5, of which 5 were waited for; matrix products, arithmetic and copies ran while one was open for 2% of the time, Pallas kernels for 0%

commit v1 on v0

--- a/solution.py
+++ b/solution.py
@@ -155,7 +155,8 @@
     local_down_weight = down_weight[0]
     arrived = lax.all_to_all(outgoing, "sp", split_axis=0, concat_axis=0, tiled=True)
     arrived_rows = arrived.reshape(-1, columns)
-    col_part = lax.all_gather(arrived_rows, "tp", axis=1, tiled=True)
+    outgoing_2 = jnp.stack([arrived_rows] * lax.axis_size("tp"))
+    col_part = jnp.concatenate(lax.all_to_all(outgoing_2, "tp", 0, 0), axis=1)
     gate_sum = jnp.dot(col_part, gate_here, preferred_element_type=jnp.float32)
     up_sum = jnp.dot(col_part, up_here, preferred_element_type=jnp.float32)
     slot_shape = arrived.shape

time: 372 us -> 392 us (1.054)
  blocking collectives: 82.6 us -> 147 us
  waiting for transfers between devices: 163 us -> 125 us
  starting transfers between devices: 25.7 us -> 19.6 us
    all_to_all x0 -> x1, blocking collectives: none -> 66.9 us  [local(): col_part = jnp.concatenate(lax.all_to_all(outgoing_2, 'tp', 0, 0), axis=1)]
    all_gather x1 -> x0, waiting for transfers between devices: 38.1 us -> none  [local(): col_part = lax.all_gather(arrived_rows, 'tp', axis=1, tiled=True)]
    all_to_all x1, starting transfers between devices: 9.9 us -> 3.87 us  [local(): lax.all_to_all(returned, 'sp', split_axis=0, concat_axis=0, tiled=True)]
  transfers between devices with their start and end apart: 5 -> 4, of which waited for: 5 -> 4; matrix products, arithmetic and copies ran while one was open for 2% -> 2% of each run, Pallas kernels for 0% -> 0%
where the time goes in v1:
time: 392 us; the launch traced here: 390 us
  blocking collectives  147 us (38%)
  waiting for transfers between devices  125 us (32%)
  matrix products  35.3 us (9%)
  local copies, waits for them, and re-layouts  30.8 us (8%)
  starting transfers between devices  19.6 us (5%)
  other arithmetic  19 us (5%)
  between operations  13.6 us (3%)
    all_gather x1, waiting for transfers between devices, in_one_piece(): lax.all_gather(both, axis, axis=dim, tiled=True)  86 us
    all_to_all x1, blocking collectives, local(): col_part = jnp.concatenate(lax.all_to_all(outgoing_2, 'tp', 0, 0), axis=1)  66.9 us
    all_to_all x1, blocking collectives, sum_at_owner(): lax.all_to_all(tiles, axis, split_axis=0, concat_axis=0, tiled=True)  64.9 us
    all_to_all x1, waiting for transfers between devices, sum_at_owner(): lax.all_to_all(tiles, axis, split_axis=0, concat_axis=0, tiled=True)  23.2 us
    dot_general x8, matrix products, attend_block(): jnp.einsum('hqk,hkd->hqd', weights.astype(jnp.bfloat16), value_rows, pref...  16.2 us
    all_to_all x1, blocking collectives, local(): lax.all_to_all(outgoing, 'sp', split_axis=0, concat_axis=0, tiled=True)  15.5 us
    all_to_all x1, starting transfers between devices, sum_at_owner(): lax.all_to_all(tiles, axis, split_axis=0, concat_axis=0, tiled=True)  12.3 us
    all_to_all x1, waiting for transfers between devices, local(): lax.all_to_all(returned, 'sp', split_axis=0, concat_axis=0, tiled=True)  11.3 us
  transfers between devices with their start and end apart: 4, of which 4 were waited for; matrix products, arithmetic and copies ran while one was open for 2% of the time, Pallas kernels for 0%

profile of v1, /device:TPU:1, one launch (start us, length us, event | category | flops | bytes accessed | tf_op | source)
XLA Modules:
  0.0 390.4 jit_solution(9431400826930052654)
XLA Ops:
  9.1 86.0 %all-gather.2.cloned.1.call-done = bf16[8192,128]{1,0:T(8,128)(2,1)} async-done(((bf16[256,128]{1,0:T(8,128)(2,1)}), bf16[8192,128]{1,0:T(8,128)(2,1)}) %all-gather.2.cloned.1.call-update) | async-done | bytes 2097168 | tf_op jit(solution)/shard_map/all_gather | solution.py:17
  95.1 49.2 %conditional.1 = (f32[1,256]{1,0:T(1,128)}, f32[1,256,64]{1,2,0:T(8,128)}) conditional(s32[]{:T(128)} %convert_element_type.51, () %tuple.31, (bf16[8192,128]{1,0:T(8,128)(2,1)}, bf16[256,64]{0,1:T(8,128)(2,1)}, s32[]{:T(128)}, f32[1,8192]{1,0:T(1,128)}) %tuple.32), branch_computations={%region_0.0_spmd, %region_1.6_spmd} | conditional | flops 70830592 | bytes 8277405 | solution.py:121
  95.9 5.0 %fusion.45 = (bf16[8192,64]{1,0:T(8,128)(2,1)}, bf16[8192,64]{1,0:T(8,128)(2,1)}) fusion(bf16[8192,128]{1,0:T(8,128)(2,1)} %get-tuple-element.217), kind=kLoop, calls=%fused_computation.87 | loop fusion | bytes 4194304 | tf_op jit(solution)/shard_map/split | solution.py:17
  101.0 43.3 %while.20 = (s32[]{:T(128)}, f32[1,256]{1,0:T(1,128)S(1)}, f32[1,256]{1,0:T(1,128)}, f32[1,256,64]{1,2,0:T(8,128)}, s32[]{:T(128)}, /*index=5*/bf16[8192,64]{1,0...) while((s32[]{:T(128)}, f32[1,256]{1,0:T(1,128)S(1)}, ...), condition=%wide.region_5.5_spmd.clone, body=%wide.region_2.4_spmd.clone.sunk | while | flops 70830592 | bytes 3884243 | solution.py:119
  103.9 2.0 fusion.62
  109.3 2.0 fusion.62
  112.1 1.4 fusion.58
  114.8 2.0 fusion.62
  117.6 1.4 fusion.58
  120.3 2.0 fusion.62
  125.8 2.0 fusion.62
  131.3 2.0 fusion.62
  134.0 1.4 fusion.58
  136.8 2.0 fusion.62
  142.2 2.0 fusion.62
  146.8 12.3 %all-to-all-start = ((bf16[16,256,128]{2,1,0:T(8,128)(2,1)}), bf16[16,256,128]{2,1,0:T(8,128)(2,1)S(1)}, u32[]{:S(2)}, u32[]{:S(2)}) async-start(bf16[16,256,128]{2,1,0:T(8,128)(2,1)} %bitcast.77), calls=%async_computation | async-start | bytes 2097152 | tf_op jit(solution)/shard_map/all_to_all | solution.py:27
  161.5 2.4 scatter_custom_fusion.1
  164.0 23.2 %all-to-all-done = bf16[16,256,128]{2,1,0:T(8,128)(2,1)S(1)} async-done(((bf16[16,256,128]{2,1,0:T(8,128)(2,1)}), bf16[16,256,128]{2,1,0:T(8,128)(2,1)S(1)}, u32[]{:S(2)}, u32[]{:S(2)}) %all-to-all-start) | async-done | bytes 1048608 | tf_op jit(solution)/shard_map/all_to_all | solution.py:27
  188.9 3.4 all-to-all-start.1
  193.1 2.4 scatter_custom_fusion
  195.7 4.0 %all-to-all-done.1 = f32[16,256,1]{1,2,0:T(1,128)S(1)} async-done(((f32[16,256,1]{1,2,0:T(1,128)}), f32[16,256,1]{1,2,0:T(1,128)S(1)}, u32[]{:S(2)}, u32[]{:S(2)}) %all-to-all-start.1) | async-done | bytes 16416 | tf_op jit(solution)/shard_map/all_to_all | solution.py:33
  200.7 2.0 gather_fusion
  202.9 15.5 %all_to_all.30 = bf16[32,20,128]{2,1,0:T(8,128)(2,1)S(1)} all-to-all(bf16[32,20,128]{2,1,0:T(8,128)(2,1)S(1)} %broadcast_select_fusion.2), channel_id=1, replica_groups=mesh['sp'=32,'tp'=16] {'sp'}, dimensions={0} | all-to-all | bytes 327680 | tf_op jit(solution)/shard_map/all_to_all | solution.py:156
  218.9 66.9 %all_to_all.31 = bf16[16,640,128]{1,2,0:T(8,128)(2,1)S(1)} all-to-all(bf16[16,640,128]{1,2,0:T(8,128)(2,1)S(1)} %stack.3), channel_id=1, replica_groups=mesh['sp'=32,'tp'=16] {'tp'}, dimensions={0} | all-to-all | bytes 5242880 | tf_op jit(solution)/shard_map/all_to_all | solution.py:159
  285.9 1.5 copy-done.1
  288.6 6.1 %fusion.21 = bf16[80,16,8,128]{3,2,1,0:T(8,128)(2,1)} fusion(bf16[1,256,2048]{2,1,0:T(8,128)(2,1)S(1)} %copy-done, bf16[640,2048]{0,1:T(8,128)(2,1)} %bitcast.96, bf16[1,2048,256]{2,1,0:T(8,128)(2,1)S(1)} %copy-done.7, f32[640,256]{1,0:T(8,128)S(1)} %fusion.26), kind=kOutput, calls=%fused_computation.40 | convolution fusion | flops 1344471040 | bytes 7995392 | tf_op jit(solution)/shard_map/dot_general | solution.py:164
  294.7 2.4 copy.45
  297.1 64.9 %all_to_all.32 = bf16[16,640,128]{2,1,0:T(8,128)(2,1)} all-to-all(bf16[16,640,128]{2,1,0:T(8,128)(2,1)S(1)} %bitcast.94), channel_id=1, replica_groups=mesh['sp'=32,'tp'=16] {'tp'}, dimensions={0} | all-to-all | bytes 5242880 | tf_op jit(solution)/shard_map/all_to_all | solution.py:27
  362.1 2.1 reduce_sum.77
  364.9 3.9 all-to-all-start.5
  368.9 11.3 %all-to-all-done.5 = bf16[32,20,128]{2,1,0:T(8,128)(2,1)S(1)} async-done(((bf16[32,20,128]{2,1,0:T(8,128)(2,1)}), bf16[32,20,128]{2,1,0:T(8,128)(2,1)S(1)}, u32[]{:S(2)}, u32[]{:S(2)}) %all-to-all-start.5) | async-done | bytes 163872 | tf_op jit(solution)/shard_map/all_to_all | solution.py:167
  382.1 1.5 add_convert_fusion
  (125 shorter events, 39.4 us)
Async XLA Ops:
  6.5 281.7 %copy-start = (bf16[1,256,2048]{2,1,0:T(8,128)(2,1)S(1)}, bf16[1,256,2048]{2,1,0:T(8,128)(2,1)}, u32[]{:S(2)}) copy-start(bf16[1,256,2048]{2,1,0:T(8,128)(2,1)} %param.27) | copy-start | bytes 3145732
  6.5 88.6 %all-gather.2.cloned.1.call-start = ((), (), s32[]{:S(2)}) async-start(), calls=%async_computation.6 | async-start | bytes 2162688 | tf_op jit(solution)/shard_map/all_gather | solution.py:17
  95.1 49.2 %copy-start.2 = (bf16[64,2048]{1,0:T(8,128)(2,1)S(1)}, bf16[64,2048]{1,0:T(8,128)(2,1)}, u32[]{:S(2)}) copy-start(bf16[64,2048]{1,0:T(8,128)(2,1)} %param.20) | copy-start | bytes 786436
  95.9 5.0 %copy-start.3 = (bf16[256,64]{0,1:T(8,128)(2,1)S(1)}, bf16[256,64]{0,1:T(8,128)(2,1)}, u32[]{:S(2)}) copy-start(bf16[256,64]{0,1:T(8,128)(2,1)} %get-tuple-element.272) | copy-start | bytes 98308 | tf_op jit(solution)/shard_map/cond
  144.3 14.9 %copy-start.4 = (s32[256,2]{0,1:T(2,128)S(1)}, s32[256,2]{0,1:T(2,128)}, u32[]{:S(2)}) copy-start(s32[256,2]{0,1:T(2,128)} %param.23) | copy-start | bytes 6148
  146.8 40.3 %all-to-all-start = ((bf16[16,256,128]{2,1,0:T(8,128)(2,1)}), bf16[16,256,128]{2,1,0:T(8,128)(2,1)S(1)}, u32[]{:S(2)}, u32[]{:S(2)}) async-start(bf16[16,256,128]{2,1,0:T(8,128)(2,1)} %bitcast.77), calls=%async_computation | async-start | bytes 2097152 | tf_op jit(solution)/shard_map/all_to_all | solution.py:27
  188.9 10.8 %all-to-all-start.1 = ((f32[16,256,1]{1,2,0:T(1,128)}), f32[16,256,1]{1,2,0:T(1,128)S(1)}, u32[]{:S(2)}, u32[]{:S(2)}) async-start(f32[16,256,1]{1,2,0:T(1,128)} %broadcast_in_dim.90), calls=%async_computation.1 | async-start | bytes 32768 | tf_op jit(solution)/shard_map/all_to_all | solution.py:33
  218.9 68.4 %copy-start.6 = (bf16[1,2048,256]{2,1,0:T(8,128)(2,1)S(1)}, bf16[1,2048,256]{2,1,0:T(8,128)(2,1)}, u32[]{:S(2)}) copy-start(bf16[1,2048,256]{2,1,0:T(8,128)(2,1)} %param.25) | copy-start | bytes 3145732
  285.9 1.5 copy-start.1
  287.4 1.2 copy-start.7
  362.1 6.7 %copy-start.5 = (f32[256,2]{0,1:T(2,128)S(1)}, f32[256,2]{0,1:T(2,128)}, u32[]{:S(2)}) copy-start(f32[256,2]{0,1:T(2,128)} %param.24) | copy-start | bytes 6148
  364.9 15.4 %all-to-all-start.5 = ((bf16[32,20,128]{2,1,0:T(8,128)(2,1)}), bf16[32,20,128]{2,1,0:T(8,128)(2,1)S(1)}, u32[]{:S(2)}, u32[]{:S(2)}) async-start(bf16[32,20,128]{2,1,0:T(8,128)(2,1)} %reshape.162), calls=%async_computation.5 | async-start | bytes 393216 | tf_op jit(solution)/shard_map/all_to_all | solution.py:167
Sparse Core Ops, SparseCore 0:
  10.5 84.5 all-gather.1
